TPU v7x, 32 devices: a whole 2x2x4 slice. The times are simulated.
32 devices in a mesh: rep: 8 (over z, y), fs: 2 (over core), tp: 2 (over x).
Axes of the slice: x: 2, y: 2, z: 4, core: 2. Of those that a mesh axis runs over, the one named last changes fastest.
Arguments:
- inputs: bfloat16 [2048, 2048], P(('rep', 'fs'), 'tp'), may hold values from -6 to 6
- cotangent: bfloat16 [2048, 2048], P(('rep', 'fs'), 'tp'), may hold values from -6 to 6
- w_up: bfloat16 [2048, 4096], P('fs', 'tp'), may hold values from -0.125 to 0.125
- w_down: bfloat16 [4096, 2048], P('tp', 'fs'), may hold values from -0.09375 to 0.09375
Outputs:
- grad_inputs: bfloat16 [2048, 2048], P(('rep', 'fs'), 'tp')
- grad_up: float32 [2048, 4096], P('fs', 'tp')
- grad_down: float32 [4096, 2048], P('tp', 'fs')
All inputs are finite; a program needn't handle non-finite values.
Results may differ from a plain program's by a relative error of at most 0.011.
Values may be sent and summed in bfloat16 or wider, within the bound.
A program may use at most 128 MiB of HBM per device.

v0:
```python
import functools

import jax
import jax.numpy as jnp
from jax import lax
from jax.experimental import pallas as pl
from jax.experimental.pallas import tpu as pltpu
from jax.sharding import PartitionSpec as P

MESH = pl.DeviceIdType.MESH
X, Y, UP, DOWN = range(4)
PAIR = 2


def contract_rows(left, right):
    return lax.dot_general(
        left, right, (((0,), (0,)), ((), ())), preferred_element_type=jnp.float32
    )


def contract_cols(left, right):
    return lax.dot_general(
        left, right, (((1,), (1,)), ((), ())), preferred_element_type=jnp.float32
    )


def nearest(z, depth, index):
    near = jnp.minimum(z, depth - 1 - z)
    away = (index + 1) // 2
    around = z - away if index % 2 else z + away
    outward = jnp.where(z < depth - 1 - z, z + (index - near), z - (index - near))
    return jnp.where(index <= 2 * near, around, outward)


def hidden_kernel(reps, x_ref, c_ref, up_ref, down_ref,
                  pg_out, sq_out, x_out, c_out, mine_out, theirs_out,
                  gx, gc, up, down, pg, sq,
                  send_sem, recv_sem, swap_sem, own_sem, pair_send, pair_recv, out_sem):
    rep, fs, tp = lax.axis_index("rep"), lax.axis_index("fs"), lax.axis_index("tp")
    z, y = rep // PAIR, rep % PAIR
    depth = reps // PAIR
    height = x_ref.shape[0]
    half = height // 2
    plane = PAIR * height
    hidden = up.shape[2]
    target = {
        X: {"tp": 1 - tp},
        Y: {"rep": z * PAIR + (1 - y)},
        UP: {"rep": jnp.minimum(z + 1, depth - 1) * PAIR + y},
        DOWN: {"rep": jnp.maximum(z - 1, 0) * PAIR + y},
    }
    sibling = {"fs": 1 - fs}

    def when(condition, body):
        if condition is True:
            body()
        else:
            pl.when(condition)(body)

    barrier = pltpu.get_barrier_semaphore()

    def greet(device):
        pl.semaphore_signal(barrier, inc=1, device_id=device, device_id_type=MESH)

    greet(target[X])
    greet(target[Y])
    greet(sibling)
    when(z < depth - 1, lambda: greet(target[UP]))
    when(z > 0, lambda: greet(target[DOWN]))
    pl.semaphore_wait(barrier, 3 + (z < depth - 1).astype(jnp.int32) + (z > 0).astype(jnp.int32))

    def token(core, source, extra=0):
        return pl.multiple_of((core * reps + source) * height + extra, half)

    def copy(way, sub, at, own=False):
        at_z, at_y, at_t = at
        array, part = sub
        source = at_z * PAIR + at_y
        there = (gx, gc)[array].at[(at_t + fs) % 2, pl.ds(token(fs, source, part * half), half)]
        here = (x_ref, c_ref)[array].at[pl.ds(part * half, half)] if own else there
        index, piece = array * 2 + part, source * 2 + at_t
        return pltpu.make_async_remote_copy(
            src_ref=here, dst_ref=there,
            send_sem=send_sem.at[way, index, piece],
            recv_sem=recv_sem.at[index, piece],
            device_id=target[way], device_id_type=MESH,
        )

    started, locals_started = [], []

    def start(way, sub, at, condition=True, own=False):
        when(condition, lambda: copy(way, sub, at, own).start())
        started.append((way, sub, at, condition, own))

    def arrive(sub, at):
        copy(X, sub, at).wait_recv()

    def put(here, there, sem):
        moved = pltpu.make_async_copy(here, there, sem)
        moved.start()
        locals_started.append(moved)
        return moved

    subs = [(array, part) for part in range(2) for array in range(2)]
    first = [(array, 0) for array in range(2)]
    second = [(array, 1) for array in range(2)]
    planes = [nearest(z, depth, index) for index in range(depth)]

    here = (z, y, tp)
    for sub in subs:
        start(UP, sub, here, z < depth - 1, own=True)
        start(DOWN, sub, here, z > 0, own=True)
    for sub in first + second:
        start(X, sub, here, own=True)
    for sub in second + first:
        start(Y, sub, here, own=True)
    own_slot = (tp + fs) % 2
    own_rows = pl.ds(token(fs, rep), height)
    owns = [
        pltpu.make_async_copy(from_ref, into, own_sem.at[index])
        for index, (from_ref, into) in enumerate((
            (x_ref, gx.at[own_slot, own_rows]), (c_ref, gc.at[own_slot, own_rows]),
            (up_ref, up.at[0]), (down_ref, down.at[0]),
        ))
    ]
    for own in owns:
        own.start()
    swaps = [
        pltpu.make_async_remote_copy(
            src_ref=from_ref, dst_ref=into.at[1], send_sem=swap_sem.at[0, index], recv_sem=swap_sem.at[1, index],
            device_id=sibling, device_id_type=MESH,
        )
        for index, (from_ref, into) in enumerate(((up_ref, up), (down_ref, down)))
    ]
    for swap in swaps:
        swap.start()

    def from_z(index):
        at_z = planes[index]
        at = (at_z, y, tp)
        for sub in subs:
            arrive(sub, at)
            start(UP, sub, at, jnp.logical_and(at_z < z, z < depth - 1))
            start(DOWN, sub, at, jnp.logical_and(at_z > z, z > 0))
        for sub in first + second:
            start(X, sub, at)
        for sub in second + first:
            start(Y, sub, at)

    def cross(index):
        at_z = planes[index]
        for one, two in zip(first, second):
            across_x, across_y = (at_z, y, 1 - tp), (at_z, 1 - y, tp)
            arrive(one, across_x)
            start(Y, one, across_x)
            arrive(two, across_y)
            start(X, two, across_y)

    def pair_copy(index, array, slot, core):
        rows = pl.ds(token(core, planes[index] * PAIR), plane)
        held = (gx, gc)[array]
        return pltpu.make_async_remote_copy(
            src_ref=held.at[slot, rows], dst_ref=held.at[1 - slot, rows],
            send_sem=pair_send.at[array * 2 + slot, index], recv_sem=pair_recv.at[array * 2 + slot, index],
            device_id=sibling, device_id_type=MESH,
        )

    quads = [(array, slot) for array in range(2) for slot in range(2)]

    def keep(index, core, number):
        rows = pl.ds(token(core, planes[index] * PAIR), plane)
        put(gx.at[0, rows], x_out.at[rows], out_sem.at[0, number, index])
        put(gc.at[0, rows], c_out.at[rows], out_sem.at[1, number, index])

    def rest(index):
        at_z = planes[index]
        for one, two in zip(first, second):
            arrive(one, (at_z, 1 - y, tp))
            arrive(two, (at_z, y, 1 - tp))
        for sub in subs:
            arrive(sub, (at_z, 1 - y, 1 - tp))
        for array, slot in quads:
            pair_copy(index, array, slot, fs).start()
        keep(index, fs, 0)

    def compute(index, core, number):
        rows = pl.ds(token(core, planes[index] * PAIR), plane)
        tile = hidden // 4

        @pl.loop(0, hidden // tile)
        def _(step):
            cols = pl.ds(pl.multiple_of(step * tile, tile), tile)
            preact = (
                jnp.dot(gx[0, rows, :], up[0, :, cols], preferred_element_type=jnp.float32)
                + jnp.dot(gx[1, rows, :], up[1, :, cols], preferred_element_type=jnp.float32)
            )
            act_grad = contract_cols(gc[0, rows, :], down[0, cols, :]) + contract_cols(gc[1, rows, :], down[1, cols, :])
            relu_pre = jnp.maximum(preact, 0.0)
            sq[rows, cols] = (relu_pre * relu_pre).astype(sq.dtype)
            pg[rows, cols] = (2.0 * relu_pre * act_grad).astype(pg.dtype)

        put(pg.at[rows], pg_out.at[rows], out_sem.at[2, number, index])
        put(sq.at[rows], sq_out.at[rows], out_sem.at[3, number, index])

    def compute_other(index):
        for array, slot in quads:
            pair_copy(index, array, slot, 1 - fs).wait_recv()
        keep(index, 1 - fs, 1)
        compute(index, 1 - fs, 1)

    def partial():
        width = mine_out.shape[1]
        tile = width // 4

        @pl.loop(0, width // tile)
        def _(step):
            cols = pl.ds(pl.multiple_of(step * tile, tile), tile)
            for slot, into in ((own_slot, mine_out), (1 - own_slot, theirs_out)):
                into[:, cols] = contract_cols(pg[own_rows, :], up[slot, cols, :]).astype(into.dtype)

    cross(0)
    for index in range(1, min(3, depth)):
        from_z(index)
    for own in owns:
        own.wait()
    rest(0)
    for swap in swaps:
        swap.wait()
    compute(0, fs, 0)
    for index in range(3, depth):
        from_z(index)
    if depth > 1:
        cross(1)
    compute_other(0)
    for index in range(2, depth):
        rest(index - 1)
        compute(index - 1, fs, 0)
        cross(index)
        if index == 2:
            partial()
        compute_other(index - 1)
    if depth <= 2:
        partial()
    if depth > 1:
        rest(depth - 1)
        compute(depth - 1, fs, 0)
        compute_other(depth - 1)
    for way, sub, at, condition, own in started:
        when(condition, lambda: copy(way, sub, at, own).wait_send())
    for index in range(depth):
        for array, slot in quads:
            pair_copy(index, array, slot, fs).wait_send()
    for moved in locals_started:
        moved.wait()


def hidden_gradients(reps, inputs, cotangent, w_up, w_down):
    rows, cols = inputs.shape
    hidden = w_up.shape[1]
    tokens, depth = 2 * reps * rows, reps // PAIR
    low = inputs.dtype
    anywhere, vmem = pl.BlockSpec(memory_space=pl.ANY), pl.BlockSpec(memory_space=pltpu.VMEM)
    whole, wide, part = (tokens, cols), (tokens, hidden), (rows, cols)
    flops = 8 * tokens * cols * 2 * hidden
    return pl.pallas_call(
        functools.partial(hidden_kernel, reps),
        out_shape=[jax.ShapeDtypeStruct(shape, low) for shape in (wide, wide, whole, whole, part, part)],
        in_specs=[vmem, vmem, anywhere, anywhere],
        out_specs=[anywhere] * 4 + [vmem] * 2,
        scratch_shapes=[
            pltpu.VMEM((2,) + whole, low),
            pltpu.VMEM((2,) + whole, low),
            pltpu.VMEM((2,) + w_up.shape, low),
            pltpu.VMEM((2,) + w_down.shape, low),
            pltpu.VMEM(wide, low),
            pltpu.VMEM(wide, low),
            pltpu.SemaphoreType.DMA((4, 4, reps * 2)),
            pltpu.SemaphoreType.DMA((4, reps * 2)),
            pltpu.SemaphoreType.DMA((2, 2)),
            pltpu.SemaphoreType.DMA((4,)),
            pltpu.SemaphoreType.DMA((4, depth)),
            pltpu.SemaphoreType.DMA((4, depth)),
            pltpu.SemaphoreType.DMA((4, 2, depth)),
        ],
        cost_estimate=pl.CostEstimate(flops=flops, bytes_accessed=tokens * hidden * 8, transcendentals=0),
        compiler_params=pltpu.CompilerParams(
            collective_id=0, has_side_effects=True, vmem_limit_bytes=60 * 1024 * 1024
        ),
    )(inputs, cotangent, w_up, w_down)


def few_tokens(reps, inputs, cotangent, w_up, w_down):
    pre_grad, squared, cols_in, cols_cot, mine, theirs = hidden_gradients(reps, inputs, cotangent, w_up, w_down)
    theirs = lax.ppermute(theirs, "tp", [(0, 1), (1, 0)])
    grad_up = contract_rows(cols_in, pre_grad)
    grad_down = contract_rows(squared, cols_cot)
    grad_inputs = (mine.astype(jnp.float32) + theirs.astype(jnp.float32)).astype(jnp.bfloat16)
    return grad_inputs, grad_up, grad_down


def many_tokens(inputs, cotangent, w_up, w_down):
    rows_in, rows_cot = (
        lax.all_gather(inputs, "tp", axis=1, tiled=True),
        lax.all_gather(cotangent, "tp", axis=1, tiled=True),
    )
    cols_in, cols_cot = (
        lax.all_to_all(rows_in, "fs", split_axis=1, concat_axis=0, tiled=True),
        lax.all_to_all(rows_cot, "fs", split_axis=1, concat_axis=0, tiled=True),
    )
    full_up, full_down = (
        lax.all_gather(w_up, "fs", axis=0, tiled=True),
        lax.all_gather(w_down, "fs", axis=1, tiled=True),
    )
    act_grad = contract_cols(rows_cot, full_down)
    preact = jnp.dot(rows_in, full_up, preferred_element_type=jnp.float32)
    relu_pre = jnp.maximum(preact, 0.0)
    squared = (relu_pre * relu_pre).astype(jnp.bfloat16)
    pre_grad = (2.0 * relu_pre * act_grad).astype(jnp.bfloat16)
    partial_value = contract_cols(pre_grad, full_up)
    grad_inputs = lax.psum_scatter(
        partial_value.astype(jnp.bfloat16), "tp", scatter_dimension=1, tiled=True
    )
    grad_piece = lax.all_gather(pre_grad, "fs", axis=0, tiled=True)
    square_piece = lax.all_gather(squared, "fs", axis=0, tiled=True)
    local_up = contract_rows(cols_in, grad_piece)
    local_down = contract_rows(square_piece, cols_cot)
    slice_up = lax.psum_scatter(local_up, "rep", scatter_dimension=0, tiled=True)
    slice_down = lax.psum_scatter(local_down, "rep", scatter_dimension=0, tiled=True)
    grad_up = lax.all_gather(slice_up, "rep", axis=0, tiled=True)
    grad_down = lax.all_gather(slice_down, "rep", axis=0, tiled=True)
    return (grad_inputs, grad_up, grad_down)


def solution(mesh):
    reps, n_fs, n_tp = mesh.shape["rep"], mesh.shape["fs"], mesh.shape["tp"]

    def shards(inputs, cotangent, w_up, w_down):
        gathered = 2 * reps * n_tp * inputs.size * inputs.dtype.itemsize
        gradients = (w_up.size + w_down.size) * 4
        fits = n_fs == 2 and n_tp == 2 and reps % PAIR == 0 and inputs.shape[0] % 32 == 0
        if fits and gathered <= gradients:
            return few_tokens(reps, inputs, cotangent, w_up, w_down)
        return many_tokens(inputs, cotangent, w_up, w_down)

    return jax.shard_map(
        shards,
        mesh=mesh,
        in_specs=(P(("rep", "fs"), "tp"), P(("rep", "fs"), "tp"), P("fs", "tp"), P("tp", "fs")),
        out_specs=(P(("rep", "fs"), "tp"), P("fs", "tp"), P("tp", "fs")),
        check_vma=False,
    )
```

profile of v0, /device:TPU:0, one launch (start us, length us, event | category | flops | bytes accessed | tf_op | source)
XLA Modules:
  0.0 131.8 jit_solution(3358375556223587038)
XLA Ops:
  0.6 103.4 %shard_map.67 = (bf16[2048,2048]{1,0:T(8,128)(2,1)}, bf16[2048,2048]{1,0:T(8,128)(2,1)}, bf16[2048,1024]{1,0:T(8,128)(2,1)}, bf16[2048,1024]{1,0:T(8,128)(2,1)},...) custom-call(bf16[128,1024]{1,0:T(8,128)(2,1)} %x_ref.1, bf16[128,1024]{1,0:T(8,128)(2,1)} %c_ref.1, ...), custom_call_target="tpu_custom_call" | custom-call | flops 68719476736 | bytes 33554432 | tf_op jit(solution)/shard_map/pallas_call | solution.py:265
  104.1 0.6 collective-permute-start
  104.7 0.0 copy-start.1
  104.7 0.0 copy-start.2
  104.7 14.8 %fusion = f32[1024,2048]{1,0:T(8,128)} fusion(bf16[2048,1024]{1,0:T(8,128)(2,1)} %get-tuple-element.11, bf16[2048,2048]{1,0:T(8,128)(2,1)} %get-tuple-element.12), kind=kOutput, calls=%fused_computation.1 | convolution fusion | flops 8589934592 | bytes 20971520 | tf_op jit(solution)/shard_map/dot_general | solution.py:16
  119.4 0.0 copy-done.1
  119.4 0.0 copy-done.2
  119.4 0.0 copy-start
  119.4 11.6 %fusion.1 = f32[2048,1024]{1,0:T(8,128)} fusion(bf16[2048,2048]{1,0:T(8,128)(2,1)S(1)} %copy-done.1, bf16[2048,1024]{1,0:T(8,128)(2,1)S(1)} %copy-done.2), kind=kOutput, calls=%fused_computation.2 | convolution fusion | flops 8589934592 | bytes 20971520 | tf_op jit(solution)/shard_map/dot_general | solution.py:16
  131.0 0.0 collective-permute-done
  131.0 0.0 copy-done
  131.0 0.8 add_convert_fusion
Async XLA Ops:
  104.1 26.9 %collective-permute-start = (bf16[128,1024]{1,0:T(8,128)(2,1)}, bf16[128,1024]{1,0:T(8,128)(2,1)S(1)}, u32[]{:S(2)}, u32[]{:S(2)}) collective-permute-start(bf16[128,1024]{1,0:T(8,128)(2,1)} %get-tuple-element.10), channel_id=1, source_target_pairs={{0,1},{1,0},{2,3},{3,2},{4,5},{5,4},{6,7},{7,6},{8,9},{9,8},{10,11... | collective-permute-start | bytes 786440 | tf_op jit(solution)/shard_map/ppermute | solution.py:294
  104.7 14.8 %copy-start.1 = (bf16[2048,2048]{1,0:T(8,128)(2,1)S(1)}, bf16[2048,2048]{1,0:T(8,128)(2,1)}, u32[]{:S(2)}) copy-start(bf16[2048,2048]{1,0:T(8,128)(2,1)} %get-tuple-element.13) | copy-start | bytes 25165828
  104.7 14.8 %copy-start.2 = (bf16[2048,1024]{1,0:T(8,128)(2,1)S(1)}, bf16[2048,1024]{1,0:T(8,128)(2,1)}, u32[]{:S(2)}) copy-start(bf16[2048,1024]{1,0:T(8,128)(2,1)} %get-tuple-element.14) | copy-start | bytes 12582916
  119.4 11.6 %copy-start = (bf16[128,1024]{1,0:T(8,128)(2,1)S(1)}, bf16[128,1024]{1,0:T(8,128)(2,1)}, u32[]{:S(2)}) copy-start(bf16[128,1024]{1,0:T(8,128)(2,1)} %get-tuple-element.9) | copy-start | bytes 786436
where the time goes:
time: 132 us
  Pallas kernels  103 us (78%)
  matrix products  26.3 us (20%)
    pallas_call x1, Pallas kernels, hidden_gradients(): pl.pallas_call(functools.partial(hidden_kernel, reps), out_shape=[jax.Sha...  103 us
    dot_general x2, matrix products, contract_rows(): lax.dot_general(left, right, (((0,), (0,)), ((), ())), preferred_element_...  26.3 us
  transfers between devices with their start and end apart: 1, of which 0 were waited for; matrix products, arithmetic and copies ran while one was open for 20% of the time, Pallas kernels for 0%

commit v1 on v0

v1 whole, which is shorter than its diff:
```python
import functools

import jax
import jax.numpy as jnp
from jax import lax
from jax.experimental import pallas as pl
from jax.experimental.pallas import tpu as pltpu
from jax.sharding import PartitionSpec as P

MESH = pl.DeviceIdType.MESH
X, Y, UP, DOWN = range(4)
PAIR = 2
OWN, SIBLING, OTHER = range(3)
PLACES = (0, 1, 2, 3, 0, 1, 4, 5)
GRANT = 22 * 1024 * 1024


def contract_rows(left, right):
    return lax.dot_general(
        left, right, (((0,), (0,)), ((), ())), preferred_element_type=jnp.float32
    )


def contract_cols(left, right):
    return lax.dot_general(
        left, right, (((1,), (1,)), ((), ())), preferred_element_type=jnp.float32
    )


def nearest(z, depth, index):
    near = jnp.minimum(z, depth - 1 - z)
    away = (index + 1) // 2
    around = z - away if index % 2 else z + away
    outward = jnp.where(z < depth - 1 - z, z + (index - near), z - (index - near))
    return jnp.where(index <= 2 * near, around, outward)


def hidden_kernel(reps, x_ref, c_ref, up_ref, down_ref,
                  acc_up, acc_down, gx, gc, pg, sq, mine, theirs,
                  up, down, stage, sent,
                  free_sem, send_sem, recv_sem, swap_sem, turn_sem, own_sem, stage_sem,
                  pair_send, pair_recv, part_sem):
    rep, fs, tp = lax.axis_index("rep"), lax.axis_index("fs"), lax.axis_index("tp")
    z, y = rep // PAIR, rep % PAIR
    depth = reps // PAIR
    height, width = x_ref.shape
    half = height // 2
    hidden = up.shape[2]
    reach = depth - 2
    target = {
        X: {"tp": 1 - tp},
        Y: {"rep": z * PAIR + (1 - y)},
        UP: {"rep": jnp.minimum(z + 1, depth - 1) * PAIR + y},
        DOWN: {"rep": jnp.maximum(z - 1, 0) * PAIR + y},
    }
    sibling = {"fs": 1 - fs}
    above, below = z < depth - 1, z > 0
    planes = [nearest(z, depth, index) for index in range(depth)]
    own_block = ((tp + fs) % 2) * OTHER

    chunk = stage.shape[1]
    chunks = down_ref.shape[0] // chunk

    def stage_copy(number):
        rows = pl.ds(number * chunk, chunk)
        return pltpu.make_async_copy(down_ref.at[rows], stage.at[number % 2], stage_sem.at[number % 2])

    owns = [
        pltpu.make_async_copy(x_ref, gx.at[rep, own_block], own_sem.at[0]),
        pltpu.make_async_copy(c_ref, gc.at[rep, own_block], own_sem.at[1]),
    ]
    for own in owns:
        own.start()
    stage_copy(0).start()
    stage_copy(1).start()
    own_up = pltpu.make_async_copy(up_ref, up.at[0], own_sem.at[2])
    own_up.start()

    barrier = pltpu.get_barrier_semaphore()

    def greet(device):
        pl.semaphore_signal(barrier, inc=1, device_id=device, device_id_type=MESH)

    greet(target[X])
    greet(target[Y])
    greet(sibling)
    pl.when(above)(lambda: greet(target[UP]))
    pl.when(below)(lambda: greet(target[DOWN]))
    pl.semaphore_wait(barrier, 3 + above.astype(jnp.int32) + below.astype(jnp.int32))

    started = []

    def copy(way, sub, at):
        at_z, at_y, at_t = at
        array, part = sub
        unit = at_z * PAIR + at_y
        place = (gx, gc)[array].at[unit, ((at_t + fs) % 2) * OTHER, pl.ds(part * half, half)]
        index, piece = array * 2 + part, unit * 2 + at_t
        return pltpu.make_async_remote_copy(
            src_ref=place, dst_ref=place,
            send_sem=send_sem.at[way, index, piece], recv_sem=recv_sem.at[index, piece],
            device_id=target[way], device_id_type=MESH,
        )

    def start(way, sub, at, condition=None):
        if condition is None:
            copy(way, sub, at).start()
        else:
            pl.when(condition)(lambda: copy(way, sub, at).start())
        started.append((way, sub, at, condition))

    def arrive(sub, at, condition=None):
        if condition is None:
            copy(X, sub, at).wait_recv()
        else:
            pl.when(condition)(lambda: copy(X, sub, at).wait_recv())

    first = [(array, 0) for array in range(2)]
    second = [(array, 1) for array in range(2)]
    subs = first + second
    far_y, far_x = subs[:3], subs[3:]

    def sides(distance):
        return (
            (z - distance, z >= distance, UP, jnp.logical_and(z >= distance, above)),
            (z + distance, z + distance < depth, DOWN, jnp.logical_and(z + distance < depth, below)),
        )

    def column(distance, sub):
        for at_z, there, way, onward in sides(distance):
            at = (at_z, y, tp)
            arrive(sub, at, there)
            start(way, sub, at, onward)
            start(X, sub, at, there)
            start(Y, sub, at, there)

    def cross(one, two):
        arrive(one, (z, y, 1 - tp))
        start(Y, one, (z, y, 1 - tp))
        arrive(two, (z, 1 - y, tp))
        start(X, two, (z, 1 - y, tp))

    def corner_own(sub):
        at = (z, 1 - y, 1 - tp)
        arrive(sub, at)
        start(UP, sub, at, above)
        start(DOWN, sub, at, below)

    def corner(distance, sub):
        for at_z, there, way, onward in sides(distance):
            at = (at_z, 1 - y, 1 - tp)
            arrive(sub, at, there)
            if distance < reach:
                start(way, sub, at, onward)

    last = planes[depth - 1]
    far = jnp.logical_or(last - z > reach, z - last > reach)

    def far_cross(sub):
        if sub in far_y:
            arrive(sub, (last, y, 1 - tp))
            start(Y, sub, (last, y, 1 - tp), far)
        else:
            arrive(sub, (last, 1 - y, tp))
            start(X, sub, (last, 1 - y, tp), far)

    def unit_of(index, row):
        return planes[index] * PAIR + row

    turns = [(0, y), (0, 1 - y), (1, y), (1, 1 - y), (2, y), (3, y), (2, 1 - y), (3, 1 - y)]

    def pair_copy(array, turn):
        held = (gx, gc, pg, sq)[array]
        at, source = (unit_of(*turns[turn]), OTHER) if array < 2 else (PLACES[turn], OWN)
        return pltpu.make_async_remote_copy(
            src_ref=held.at[at, source], dst_ref=held.at[at, SIBLING],
            send_sem=pair_send.at[array, turn], recv_sem=pair_recv.at[array, turn],
            device_id=sibling, device_id_type=MESH,
        )

    def ready_same(index, turn):
        done = first if index == 0 else far_y if index == depth - 1 else []
        for sub in subs:
            if sub not in done:
                arrive(sub, (planes[index], y, 1 - tp))
        for array in range(2):
            pair_copy(array, turn).start()

    def ready_other(index, turn):
        done = second if index == 0 else far_x if index == depth - 1 else []
        for sub in subs:
            if sub not in done:
                arrive(sub, (planes[index], 1 - y, tp))
        if index == depth - 1:
            for sub in subs:
                arrive(sub, (last, 1 - y, 1 - tp), far)
        for array in range(2):
            pair_copy(array, turn).start()

    def compute(turn):
        unit, place = unit_of(*turns[turn]), PLACES[turn]
        tile = hidden // 4

        @pl.loop(0, hidden // tile)
        def _(step):
            cols = pl.ds(pl.multiple_of(step * tile, tile), tile)
            preact = (
                jnp.dot(gx[unit, OWN], up[0, :, cols], preferred_element_type=jnp.float32)
                + jnp.dot(gx[unit, OTHER], up[1, :, cols], preferred_element_type=jnp.float32)
            )
            act_grad = (
                jnp.dot(gc[unit, OWN], down[0, :, cols], preferred_element_type=jnp.float32)
                + jnp.dot(gc[unit, OTHER], down[1, :, cols], preferred_element_type=jnp.float32)
            )
            relu_pre = jnp.maximum(preact, 0.0)
            sq[place, OWN, :, cols] = (relu_pre * relu_pre).astype(sq.dtype)
            pg[place, OWN, :, cols] = (2.0 * relu_pre * act_grad).astype(pg.dtype)

        for array in (2, 3):
            pair_copy(array, turn).start()

    def both(ref, unit, cols):
        block = ref[unit, pl.ds(OWN, 2), :, cols]
        return block.reshape(2 * height, block.shape[2])

    def gather_pair(first_turn):
        for turn in (first_turn, first_turn + 1):
            for array in range(4):
                pair_copy(array, turn).wait_recv()

    def weight_grad(first_turn, into, left, right):
        rows, cols = into.shape
        span, tile = width, 256
        pair = (first_turn, first_turn + 1)

        def block(ref, turn, cols):
            return both(ref, unit_of(*turns[turn]) if ref is gx or ref is gc else PLACES[turn], cols)

        @pl.loop(0, (rows // span) * (cols // tile))
        def _(step):
            at = pl.ds(pl.multiple_of((step // (cols // tile)) * span, span), span)
            across = pl.ds(pl.multiple_of((step % (cols // tile)) * tile, tile), tile)
            total = sum(contract_rows(block(left, turn, at), block(right, turn, across)) for turn in pair)
            into[at, across] = total if first_turn == 0 else into[at, across] + total

    def partial():
        tile = width // 4

        @pl.loop(0, width // tile)
        def _(step):
            cols = pl.ds(pl.multiple_of(step * tile, tile), tile)
            for slot, into in (((tp + fs) % 2, mine), ((tp + fs + 1) % 2, sent)):
                into[:, cols] = contract_cols(pg[PLACES[0], OWN], up[slot, cols, :]).astype(into.dtype)

    part_copy = pltpu.make_async_remote_copy(
        src_ref=sent, dst_ref=theirs, send_sem=part_sem.at[0], recv_sem=part_sem.at[1],
        device_id=target[X], device_id_type=MESH,
    )
    swap_up = pltpu.make_async_remote_copy(
        src_ref=up_ref, dst_ref=up.at[1], send_sem=swap_sem.at[0], recv_sem=swap_sem.at[1],
        device_id=sibling, device_id_type=MESH,
    )

    def turn_copy(number):
        cols = pl.ds(number * chunk, chunk)
        return pltpu.make_async_remote_copy(
            src_ref=down.at[0, :, cols], dst_ref=down.at[1, :, cols],
            send_sem=turn_sem.at[0, number], recv_sem=turn_sem.at[1, number],
            device_id=sibling, device_id_type=MESH,
        )

    for own in owns:
        own.wait()
    here = (z, y, tp)
    for k, sub in enumerate(subs):
        start(UP, sub, here, above)
        start(DOWN, sub, here, below)
        start(X, sub, here)
        start(Y, (second + first)[k], here)
    swap_up.start()
    for number in range(chunks):
        stage_copy(number).wait()
        down[0, :, pl.ds(number * chunk, chunk)] = stage[number % 2].T
        if number + 2 < chunks:
            stage_copy(number + 2).start()
        turn_copy(number).start()

    cross(first[0], second[0])
    column(1, subs[0])
    cross(first[1], second[1])
    for sub in subs[1:]:
        column(1, sub)
    ready_same(0, 0)
    own_up.wait()
    swap_up.wait()
    for number in range(chunks):
        turn_copy(number).wait()
    compute(0)
    for sub in subs:
        corner_own(sub)
    for sub in subs[:2]:
        column(2, sub)
    ready_other(0, 1)
    compute(1)
    for sub in subs[2:]:
        column(2, sub)
    partial()
    gather_pair(0)
    weight_grad(0, acc_up, gx, pg)
    ready_same(1, 2)
    compute(2)
    weight_grad(0, acc_down, sq, gc)
    pl.semaphore_signal(free_sem, inc=1, device_id=sibling, device_id_type=MESH)
    for sub in subs:
        corner(1, sub)
    for sub in subs[:2]:
        column(3, sub)
    ready_other(1, 3)
    compute(3)
    for sub in subs[2:]:
        column(3, sub)
    for turn in (0, 1):
        for array in (2, 3):
            pair_copy(array, turn).wait_send()
    pl.semaphore_wait(free_sem, 1)
    gather_pair(2)
    weight_grad(2, acc_up, gx, pg)
    ready_same(2, 4)
    compute(4)
    for sub in subs:
        far_cross(sub)
    part_copy.start()
    weight_grad(2, acc_down, sq, gc)
    ready_same(3, 5)
    compute(5)
    for sub in subs:
        corner(2, sub)
    gather_pair(4)
    weight_grad(4, acc_up, gx, pg)
    ready_other(2, 6)
    compute(6)
    ready_other(3, 7)
    compute(7)
    weight_grad(4, acc_down, sq, gc)
    gather_pair(6)
    part_copy.wait()
    for way, sub, at, condition in started:
        if condition is None:
            copy(way, sub, at).wait_send()
        else:
            pl.when(condition)(functools.partial(lambda w, s, a: copy(w, s, a).wait_send(), way, sub, at))
    for turn in range(len(turns)):
        for array in range(4):
            if array < 2 or turn >= 2:
                pair_copy(array, turn).wait_send()


def finish_kernel(reps, acc_up, acc_down, gx, gc, pg, sq, mine, theirs,
                  inputs_out, up_out, down_out, tiles, added, tile_sem, added_sem):
    rep = lax.axis_index("rep")
    z, y = rep // PAIR, rep % PAIR
    depth = reps // PAIR
    units = [nearest(z, depth, index) * PAIR + (1 - y) for index in (depth - 2, depth - 1)]
    height = gx.shape[2]
    slots, span, tile = tiles.shape

    added[...] = (mine[...].astype(jnp.float32) + theirs[...].astype(jnp.float32)).astype(added.dtype)
    put = pltpu.make_async_copy(added, inputs_out, added_sem)
    put.start()

    def both(ref, unit, cols):
        block = ref[unit, pl.ds(OWN, 2), :, cols]
        return block.reshape(2 * height, block.shape[2])

    base = 0
    for held, out, left, right in ((acc_up, up_out, gx, pg), (acc_down, down_out, sq, gc)):
        rows, cols = held.shape
        across_count = cols // tile
        count = (rows // span) * across_count

        def place(step):
            return (
                pl.ds(pl.multiple_of((step // across_count) * span, span), span),
                pl.ds(pl.multiple_of((step % across_count) * tile, tile), tile),
            )

        def out_copy(step, slot):
            at, across = place(step)
            return pltpu.make_async_copy(tiles.at[slot], out.at[at, across], tile_sem.at[slot])

        @pl.loop(0, count)
        def _(step):
            slot = step % slots
            pl.when(step >= slots)(lambda: out_copy(step - slots, slot).wait())
            at, across = place(step)
            total = sum(
                contract_rows(both(left, one, at), both(right, other, across))
                for one, other in zip(*((units, PLACES[-2:]) if right is pg else (PLACES[-2:], units)))
            )
            tiles[slot] = held[at, across] + total
            out_copy(step, slot).start()

        for step in range(count - slots, count):
            out_copy(step, step % slots).wait()
    put.wait()


def few_tokens(reps, inputs, cotangent, w_up, w_down):
    height, width = inputs.shape
    hidden = w_up.shape[1]
    depth = reps // PAIR
    low, high = inputs.dtype, jnp.float32
    far, vmem = pl.BlockSpec(memory_space=pltpu.HBM), pl.BlockSpec(memory_space=pltpu.VMEM)
    blocks, rows = (reps, 3, height, width), (max(PLACES) + 1, 2, height, hidden)
    shapes = [(w_up.shape, high), (w_down.shape, high), (blocks, low), (blocks, low), (rows, low), (rows, low),
              (inputs.shape, low), (inputs.shape, low)]
    chunk = w_down.shape[0] // 8
    tokens = reps * height
    held = pl.pallas_call(
        functools.partial(hidden_kernel, reps),
        out_shape=[pltpu.VMEM(shape, dtype) for shape, dtype in shapes],
        in_specs=[far] * 4,
        out_specs=[vmem] * len(shapes),
        scratch_shapes=[
            pltpu.VMEM((2,) + w_up.shape, low),
            pltpu.VMEM((2, width, hidden), low),
            pltpu.VMEM((2, chunk, width), low),
            pltpu.VMEM(inputs.shape, low),
            pltpu.SemaphoreType.REGULAR,
            pltpu.SemaphoreType.DMA((4, 4, reps * 2)),
            pltpu.SemaphoreType.DMA((4, reps * 2)),
            pltpu.SemaphoreType.DMA((2,)),
            pltpu.SemaphoreType.DMA((2, 8)),
            pltpu.SemaphoreType.DMA((3,)),
            pltpu.SemaphoreType.DMA((2,)),
            pltpu.SemaphoreType.DMA((4, reps)),
            pltpu.SemaphoreType.DMA((4, reps)),
            pltpu.SemaphoreType.DMA((2,)),
        ],
        cost_estimate=pl.CostEstimate(flops=14 * tokens * width * hidden, bytes_accessed=w_up.size * 8, transcendentals=0),
        compiler_params=pltpu.CompilerParams(
            collective_id=0, has_side_effects=True, vmem_limit_bytes=GRANT
        ),
    )(*(pltpu.with_memory_space_constraint(value, pltpu.HBM) for value in (inputs, cotangent, w_up, w_down)))
    return pl.pallas_call(
        functools.partial(finish_kernel, reps),
        out_shape=[
            jax.ShapeDtypeStruct(inputs.shape, low),
            jax.ShapeDtypeStruct(w_up.shape, high),
            jax.ShapeDtypeStruct(w_down.shape, high),
        ],
        in_specs=[vmem] * len(shapes),
        out_specs=[far] * 3,
        scratch_shapes=[
            pltpu.VMEM((4, width, 256), high),
            pltpu.VMEM(inputs.shape, low),
            pltpu.SemaphoreType.DMA((4,)),
            pltpu.SemaphoreType.DMA,
        ],
        cost_estimate=pl.CostEstimate(flops=16 * height * width * hidden, bytes_accessed=w_up.size * 16, transcendentals=0),
        compiler_params=pltpu.CompilerParams(vmem_limit_bytes=GRANT),
    )(*(pltpu.with_memory_space_constraint(value, pltpu.VMEM) for value in held))


def many_tokens(inputs, cotangent, w_up, w_down):
    rows_in, rows_cot = (
        lax.all_gather(inputs, "tp", axis=1, tiled=True),
        lax.all_gather(cotangent, "tp", axis=1, tiled=True),
    )
    cols_in, cols_cot = (
        lax.all_to_all(rows_in, "fs", split_axis=1, concat_axis=0, tiled=True),
        lax.all_to_all(rows_cot, "fs", split_axis=1, concat_axis=0, tiled=True),
    )
    full_up, full_down = (
        lax.all_gather(w_up, "fs", axis=0, tiled=True),
        lax.all_gather(w_down, "fs", axis=1, tiled=True),
    )
    act_grad = contract_cols(rows_cot, full_down)
    preact = jnp.dot(rows_in, full_up, preferred_element_type=jnp.float32)
    relu_pre = jnp.maximum(preact, 0.0)
    squared = (relu_pre * relu_pre).astype(jnp.bfloat16)
    pre_grad = (2.0 * relu_pre * act_grad).astype(jnp.bfloat16)
    partial_value = contract_cols(pre_grad, full_up)
    grad_inputs = lax.psum_scatter(
        partial_value.astype(jnp.bfloat16), "tp", scatter_dimension=1, tiled=True
    )
    grad_piece = lax.all_gather(pre_grad, "fs", axis=0, tiled=True)
    square_piece = lax.all_gather(squared, "fs", axis=0, tiled=True)
    local_up = contract_rows(cols_in, grad_piece)
    local_down = contract_rows(square_piece, cols_cot)
    slice_up = lax.psum_scatter(local_up, "rep", scatter_dimension=0, tiled=True)
    slice_down = lax.psum_scatter(local_down, "rep", scatter_dimension=0, tiled=True)
    grad_up = lax.all_gather(slice_up, "rep", axis=0, tiled=True)
    grad_down = lax.all_gather(slice_down, "rep", axis=0, tiled=True)
    return (grad_inputs, grad_up, grad_down)


def solution(mesh):
    reps, n_fs, n_tp = mesh.shape["rep"], mesh.shape["fs"], mesh.shape["tp"]

    def shards(inputs, cotangent, w_up, w_down):
        gathered = 2 * reps * n_tp * inputs.size * inputs.dtype.itemsize
        gradients = (w_up.size + w_down.size) * 4
        fits = n_fs == 2 and n_tp == 2 and reps == PAIR * 4 and inputs.shape[0] % 32 == 0
        if fits and gathered <= gradients:
            return few_tokens(reps, inputs, cotangent, w_up, w_down)
        return many_tokens(inputs, cotangent, w_up, w_down)

    return jax.shard_map(
        shards,
        mesh=mesh,
        in_specs=(P(("rep", "fs"), "tp"), P(("rep", "fs"), "tp"), P("fs", "tp"), P("tp", "fs")),
        out_specs=(P(("rep", "fs"), "tp"), P("fs", "tp"), P("tp", "fs")),
        check_vma=False,
    )
```

time: 132 us -> 101 us (0.77)
  the two profiles are of different devices: /device:TPU:0 before, /device:TPU:8 now
where the time goes in v1:
time: 101 us
  Pallas kernels  100 us (99%)
    pallas_call x1, Pallas kernels, few_tokens(): pl.pallas_call(functools.partial(hidden_kernel, reps), out_shape=[pltpu.V...  89.4 us
    pallas_call x1, Pallas kernels, few_tokens(): pl.pallas_call(functools.partial(finish_kernel, reps), out_shape=[jax.Sha...  10.6 us

profile of v1, /device:TPU:8, one launch (start us, length us, event | category | flops | bytes accessed | tf_op | source)
XLA Modules:
  0.0 100.6 jit_solution(14929826949553447690)
XLA Ops:
  0.6 89.4 %shard_map.67 = (f32[1024,2048]{1,0:T(8,128)S(1)}, f32[2048,1024]{1,0:T(8,128)S(1)}, bf16[8,3,128,1024]{3,2,1,0:T(8,128)(2,1)S(1)}, bf16[8,3,128,1024]{3,2,1,0:T...) custom-call(bf16[128,1024]{1,0:T(8,128)(2,1)} %x_ref.1, ...), custom_call_target="tpu_custom_call" | custom-call | flops 30064771072 | bytes 16777216 | tf_op jit(solution)/shard_map/pallas_call | solution.py:419
  90.0 10.6 %shard_map.68 = (bf16[128,1024]{1,0:T(8,128)(2,1)}, f32[1024,2048]{1,0:T(8,128)}, f32[2048,1024]{1,0:T(8,128)}) custom-call(f32[1024,2048]{1,0:T(8,128)S(1)} %get-tuple-element.11.acc_up, f32[2048,1024]{1,0:T(8,128)S(1)} %get-tuple-element.12.acc_down, bf16[8,3,128,1024]{3,2,1,0:T(8,128)(2,1)S(1)} %get-tuple-element.13.gx, ...), custom_call_target="tpu_custom_call" | custom-call | flops 4294967296 | bytes 33554432 | tf_op jit(solution)/shard_map/pallas_call | solution.py:445

commit v2 on v1

--- a/solution.py
+++ b/solution.py
@@ -197,11 +197,11 @@
         for array in range(2):
             pair_copy(array, turn).start()
 
-    def compute(turn):
+    def compute(turn, lo=0, hi=2):
         unit, place = unit_of(*turns[turn]), PLACES[turn]
-        tile = hidden // 4
-
-        @pl.loop(0, hidden // tile)
+        tile = hidden // 2
+
+        @pl.loop(lo, hi)
         def _(step):
             cols = pl.ds(pl.multiple_of(step * tile, tile), tile)
             preact = (
@@ -216,8 +216,9 @@
             sq[place, OWN, :, cols] = (relu_pre * relu_pre).astype(sq.dtype)
             pg[place, OWN, :, cols] = (2.0 * relu_pre * act_grad).astype(pg.dtype)
 
-        for array in (2, 3):
-            pair_copy(array, turn).start()
+        if hi == 2:
+            for array in (2, 3):
+                pair_copy(array, turn).start()
 
     def both(ref, unit, cols):
         block = ref[unit, pl.ds(OWN, 2), :, cols]
@@ -228,20 +229,22 @@
             for array in range(4):
                 pair_copy(array, turn).wait_recv()
 
-    def weight_grad(first_turn, into, left, right):
+    def weight_grad(first_turn, into, left, right, lo=0, hi=None, parts=1):
         rows, cols = into.shape
-        span, tile = width, 256
+        span, tile = width // parts, 256
         pair = (first_turn, first_turn + 1)
 
         def block(ref, turn, cols):
             return both(ref, unit_of(*turns[turn]) if ref is gx or ref is gc else PLACES[turn], cols)
 
-        @pl.loop(0, (rows // span) * (cols // tile))
+        @pl.loop(lo, rows // span if hi is None else hi)
         def _(step):
-            at = pl.ds(pl.multiple_of((step // (cols // tile)) * span, span), span)
-            across = pl.ds(pl.multiple_of((step % (cols // tile)) * tile, tile), tile)
-            total = sum(contract_rows(block(left, turn, at), block(right, turn, across)) for turn in pair)
-            into[at, across] = total if first_turn == 0 else into[at, across] + total
+            at = pl.ds(pl.multiple_of(step * span, span), span)
+            lefts = [block(left, turn, at) for turn in pair]
+            for number in range(cols // tile):
+                across = pl.ds(number * tile, tile)
+                total = sum(contract_rows(one, block(right, turn, across)) for one, turn in zip(lefts, pair))
+                into[at, across] = total if first_turn == 0 else into[at, across] + total
 
     def partial():
         tile = width // 4
@@ -307,36 +310,42 @@
     partial()
     gather_pair(0)
     weight_grad(0, acc_up, gx, pg)
+    weight_grad(0, acc_down, sq, gc, 0, 1)
     ready_same(1, 2)
     compute(2)
-    weight_grad(0, acc_down, sq, gc)
+    weight_grad(0, acc_down, sq, gc, 1, 2)
     pl.semaphore_signal(free_sem, inc=1, device_id=sibling, device_id_type=MESH)
     for sub in subs:
         corner(1, sub)
-    for sub in subs[:2]:
-        column(3, sub)
     ready_other(1, 3)
     compute(3)
-    for sub in subs[2:]:
+    for sub in subs[:2]:
         column(3, sub)
     for turn in (0, 1):
         for array in (2, 3):
             pair_copy(array, turn).wait_send()
     pl.semaphore_wait(free_sem, 1)
     gather_pair(2)
-    weight_grad(2, acc_up, gx, pg)
+    weight_grad(2, acc_up, gx, pg, 0, 1, 2)
+    column(3, subs[2])
     ready_same(2, 4)
-    compute(4)
-    for sub in subs:
-        far_cross(sub)
+    compute(4, 0, 1)
+    column(3, subs[3])
+    compute(4, 1, 2)
+    far_cross(subs[0])
+    far_cross(subs[1])
+    weight_grad(2, acc_up, gx, pg, 1, 2, 2)
+    far_cross(subs[2])
+    weight_grad(2, acc_down, sq, gc, 0, 1)
+    far_cross(subs[3])
     part_copy.start()
-    weight_grad(2, acc_down, sq, gc)
+    weight_grad(2, acc_down, sq, gc, 1, 2)
     ready_same(3, 5)
     compute(5)
+    gather_pair(4)
+    weight_grad(4, acc_up, gx, pg)
     for sub in subs:
         corner(2, sub)
-    gather_pair(4)
-    weight_grad(4, acc_up, gx, pg)
     ready_other(2, 6)
     compute(6)
     ready_other(3, 7)
@@ -362,7 +371,8 @@
     depth = reps // PAIR
     units = [nearest(z, depth, index) * PAIR + (1 - y) for index in (depth - 2, depth - 1)]
     height = gx.shape[2]
-    slots, span, tile = tiles.shape
+    slots, span, wide = tiles.shape
+    tile = 256
 
     added[...] = (mine[...].astype(jnp.float32) + theirs[...].astype(jnp.float32)).astype(added.dtype)
     put = pltpu.make_async_copy(added, inputs_out, added_sem)
@@ -372,36 +382,24 @@
         block = ref[unit, pl.ds(OWN, 2), :, cols]
         return block.reshape(2 * height, block.shape[2])
 
-    base = 0
+    started = []
     for held, out, left, right in ((acc_up, up_out, gx, pg), (acc_down, down_out, sq, gc)):
         rows, cols = held.shape
-        across_count = cols // tile
-        count = (rows // span) * across_count
-
-        def place(step):
-            return (
-                pl.ds(pl.multiple_of((step // across_count) * span, span), span),
-                pl.ds(pl.multiple_of((step % across_count) * tile, tile), tile),
-            )
-
-        def out_copy(step, slot):
-            at, across = place(step)
-            return pltpu.make_async_copy(tiles.at[slot], out.at[at, across], tile_sem.at[slot])
-
-        @pl.loop(0, count)
-        def _(step):
-            slot = step % slots
-            pl.when(step >= slots)(lambda: out_copy(step - slots, slot).wait())
-            at, across = place(step)
-            total = sum(
-                contract_rows(both(left, one, at), both(right, other, across))
-                for one, other in zip(*((units, PLACES[-2:]) if right is pg else (PLACES[-2:], units)))
-            )
-            tiles[slot] = held[at, across] + total
-            out_copy(step, slot).start()
-
-        for step in range(count - slots, count):
-            out_copy(step, step % slots).wait()
+        pairs = list(zip(*((units, PLACES[-2:]) if right is pg else (PLACES[-2:], units))))
+        for at in (pl.ds(start, span) for start in range(0, rows, span)):
+            lefts = [both(left, one, at) for one, _ in pairs]
+            for begin in range(0, cols, wide):
+                slot = len(started) % slots
+                if len(started) >= slots:
+                    started[-slots].wait()
+                for start in range(0, wide, tile):
+                    across = pl.ds(begin + start, tile)
+                    total = sum(contract_rows(one, both(right, other, across)) for one, (_, other) in zip(lefts, pairs))
+                    tiles[slot, :, pl.ds(start, tile)] = held[at, across] + total
+                started.append(pltpu.make_async_copy(tiles.at[slot], out.at[at, pl.ds(begin, wide)], tile_sem.at[slot]))
+                started[-1].start()
+    for moved in started[-slots:]:
+        moved.wait()
     put.wait()
 
 
@@ -452,7 +450,7 @@
         in_specs=[vmem] * len(shapes),
         out_specs=[far] * 3,
         scratch_shapes=[
-            pltpu.VMEM((4, width, 256), high),
+            pltpu.VMEM((4, width, width // 2), high),
             pltpu.VMEM(inputs.shape, low),
             pltpu.SemaphoreType.DMA((4,)),
             pltpu.SemaphoreType.DMA,

time: 101 us -> 85.3 us (0.84)
  the two profiles are of different devices: /device:TPU:8 before, /device:TPU:0 now
where the time goes in v2:
time: 85.3 us; the launch traced here: 84.8 us
  Pallas kernels  84 us (98%)
    pallas_call x1, Pallas kernels, few_tokens(): pl.pallas_call(functools.partial(hidden_kernel, reps), out_shape=[pltpu.V...  77.2 us
    pallas_call x1, Pallas kernels, few_tokens(): pl.pallas_call(functools.partial(finish_kernel, reps), out_shape=[jax.Sha...  6.85 us

profile of v2, /device:TPU:0, one launch (start us, length us, event | category | flops | bytes accessed | tf_op | source)
XLA Modules:
  0.0 84.8 jit_solution(4021720438160036280)
XLA Ops:
  0.6 77.2 %shard_map.67 = (f32[1024,2048]{1,0:T(8,128)S(1)}, f32[2048,1024]{1,0:T(8,128)S(1)}, bf16[8,3,128,1024]{3,2,1,0:T(8,128)(2,1)S(1)}, bf16[8,3,128,1024]{3,2,1,0:T...) custom-call(bf16[128,1024]{1,0:T(8,128)(2,1)} %x_ref.1, ...), custom_call_target="tpu_custom_call" | custom-call | flops 30064771072 | bytes 16777216 | tf_op jit(solution)/shard_map/pallas_call | solution.py:417
  77.8 6.9 %shard_map.68 = (bf16[128,1024]{1,0:T(8,128)(2,1)}, f32[1024,2048]{1,0:T(8,128)}, f32[2048,1024]{1,0:T(8,128)}) custom-call(f32[1024,2048]{1,0:T(8,128)S(1)} %get-tuple-element.11.acc_up, f32[2048,1024]{1,0:T(8,128)S(1)} %get-tuple-element.12.acc_down, bf16[8,3,128,1024]{3,2,1,0:T(8,128)(2,1)S(1)} %get-tuple-element.13.gx, ...), custom_call_target="tpu_custom_call" | custom-call | flops 4294967296 | bytes 33554432 | tf_op jit(solution)/shard_map/pallas_call | solution.py:443

commit v3 on v2

--- a/solution.py
+++ b/solution.py
@@ -118,7 +118,7 @@
     first = [(array, 0) for array in range(2)]
     second = [(array, 1) for array in range(2)]
     subs = first + second
-    far_y, far_x = subs[:3], subs[3:]
+    far_y, far_x = first, second
 
     def sides(distance):
         return (
@@ -126,13 +126,18 @@
             (z + distance, z + distance < depth, DOWN, jnp.logical_and(z + distance < depth, below)),
         )
 
-    def column(distance, sub):
-        for at_z, there, way, onward in sides(distance):
-            at = (at_z, y, tp)
-            arrive(sub, at, there)
-            start(way, sub, at, onward)
-            start(X, sub, at, there)
-            start(Y, sub, at, there)
+    def spread(sub, side):
+        at_z, there, _, _ = side
+        start(X, sub, (at_z, y, tp), there)
+        start(Y, sub, (at_z, y, tp), there)
+
+    def column(distance, sub, defer=False):
+        for side in sides(distance):
+            at_z, there, way, onward = side
+            arrive(sub, (at_z, y, tp), there)
+            start(way, sub, (at_z, y, tp), onward)
+            if way == UP or not defer:
+                spread(sub, side)
 
     def cross(one, two):
         arrive(one, (z, y, 1 - tp))
@@ -224,15 +229,14 @@
         block = ref[unit, pl.ds(OWN, 2), :, cols]
         return block.reshape(2 * height, block.shape[2])
 
-    def gather_pair(first_turn):
-        for turn in (first_turn, first_turn + 1):
+    def gather(*several):
+        for turn in several:
             for array in range(4):
                 pair_copy(array, turn).wait_recv()
 
-    def weight_grad(first_turn, into, left, right, lo=0, hi=None, parts=1):
+    def weight_grad(several, into, left, right, lo=0, hi=None, parts=1):
         rows, cols = into.shape
         span, tile = width // parts, 256
-        pair = (first_turn, first_turn + 1)
 
         def block(ref, turn, cols):
             return both(ref, unit_of(*turns[turn]) if ref is gx or ref is gc else PLACES[turn], cols)
@@ -240,11 +244,11 @@
         @pl.loop(lo, rows // span if hi is None else hi)
         def _(step):
             at = pl.ds(pl.multiple_of(step * span, span), span)
-            lefts = [block(left, turn, at) for turn in pair]
+            lefts = [block(left, turn, at) for turn in several]
             for number in range(cols // tile):
                 across = pl.ds(number * tile, tile)
-                total = sum(contract_rows(one, block(right, turn, across)) for one, turn in zip(lefts, pair))
-                into[at, across] = total if first_turn == 0 else into[at, across] + total
+                total = sum(contract_rows(one, block(right, turn, across)) for one, turn in zip(lefts, several))
+                into[at, across] = total if 0 in several else into[at, across] + total
 
     def partial():
         tile = width // 4
@@ -289,10 +293,12 @@
         turn_copy(number).start()
 
     cross(first[0], second[0])
-    column(1, subs[0])
+    column(1, subs[0], True)
     cross(first[1], second[1])
     for sub in subs[1:]:
-        column(1, sub)
+        column(1, sub, True)
+    for sub in subs:
+        spread(sub, sides(1)[1])
     ready_same(0, 0)
     own_up.wait()
     swap_up.wait()
@@ -308,50 +314,52 @@
     for sub in subs[2:]:
         column(2, sub)
     partial()
-    gather_pair(0)
-    weight_grad(0, acc_up, gx, pg)
-    weight_grad(0, acc_down, sq, gc, 0, 1)
+    gather(0, 1)
+    weight_grad((0, 1), acc_up, gx, pg)
+    weight_grad((0, 1), acc_down, sq, gc, 0, 1)
     ready_same(1, 2)
     compute(2)
-    weight_grad(0, acc_down, sq, gc, 1, 2)
+    weight_grad((0, 1), acc_down, sq, gc, 1, 2)
     pl.semaphore_signal(free_sem, inc=1, device_id=sibling, device_id_type=MESH)
     for sub in subs:
         corner(1, sub)
     ready_other(1, 3)
     compute(3)
-    for sub in subs[:2]:
-        column(3, sub)
     for turn in (0, 1):
         for array in (2, 3):
             pair_copy(array, turn).wait_send()
     pl.semaphore_wait(free_sem, 1)
-    gather_pair(2)
-    weight_grad(2, acc_up, gx, pg, 0, 1, 2)
-    column(3, subs[2])
+    for sub in subs[:2]:
+        column(3, sub)
+    gather(2, 3)
+    weight_grad((2, 3), acc_up, gx, pg, 0, 1, 2)
     ready_same(2, 4)
     compute(4, 0, 1)
+    column(3, subs[2])
+    far_cross(subs[0])
+    compute(4, 1, 2)
     column(3, subs[3])
-    compute(4, 1, 2)
-    far_cross(subs[0])
+    weight_grad((2, 3), acc_up, gx, pg, 1, 2, 2)
     far_cross(subs[1])
-    weight_grad(2, acc_up, gx, pg, 1, 2, 2)
+    weight_grad((2, 3), acc_down, sq, gc)
     far_cross(subs[2])
-    weight_grad(2, acc_down, sq, gc, 0, 1)
+    gather(4)
+    weight_grad((4,), acc_up, gx, pg)
+    weight_grad((4,), acc_down, sq, gc)
     far_cross(subs[3])
     part_copy.start()
-    weight_grad(2, acc_down, sq, gc, 1, 2)
     ready_same(3, 5)
     compute(5)
-    gather_pair(4)
-    weight_grad(4, acc_up, gx, pg)
     for sub in subs:
         corner(2, sub)
     ready_other(2, 6)
     compute(6)
     ready_other(3, 7)
     compute(7)
-    weight_grad(4, acc_down, sq, gc)
-    gather_pair(6)
+    gather(5)
+    weight_grad((5,), acc_up, gx, pg)
+    weight_grad((5,), acc_down, sq, gc)
+    gather(6, 7)
     part_copy.wait()
     for way, sub, at, condition in started:
         if condition is None:

time: 85.3 us -> 83 us (0.973)
  Pallas kernels: 84 us -> 82 us
    pallas_call x1, Pallas kernels: 77.2 us -> 75.2 us  [few_tokens(): pl.pallas_call(functools.partial(hidden_kernel, reps), out_shape=[pltpu.V...]
where the time goes in v3:
time: 83 us; the launch traced here: 82.8 us
  Pallas kernels  82 us (99%)
    pallas_call x1, Pallas kernels, few_tokens(): pl.pallas_call(functools.partial(hidden_kernel, reps), out_shape=[pltpu.V...  75.2 us
    pallas_call x1, Pallas kernels, few_tokens(): pl.pallas_call(functools.partial(finish_kernel, reps), out_shape=[jax.Sha...  6.86 us

profile of v3, /device:TPU:0, one launch (start us, length us, event | category | flops | bytes accessed | tf_op | source)
XLA Modules:
  0.0 82.8 jit_solution(33751752502651201)
XLA Ops:
  0.6 75.2 %shard_map.67 = (f32[1024,2048]{1,0:T(8,128)S(1)}, f32[2048,1024]{1,0:T(8,128)S(1)}, bf16[8,3,128,1024]{3,2,1,0:T(8,128)(2,1)S(1)}, bf16[8,3,128,1024]{3,2,1,0:T...) custom-call(bf16[128,1024]{1,0:T(8,128)(2,1)} %x_ref.1, ...), custom_call_target="tpu_custom_call" | custom-call | flops 30064771072 | bytes 16777216 | tf_op jit(solution)/shard_map/pallas_call | solution.py:425
  75.8 6.9 %shard_map.68 = (bf16[128,1024]{1,0:T(8,128)(2,1)}, f32[1024,2048]{1,0:T(8,128)}, f32[2048,1024]{1,0:T(8,128)}) custom-call(f32[1024,2048]{1,0:T(8,128)S(1)} %get-tuple-element.11.acc_up, f32[2048,1024]{1,0:T(8,128)S(1)} %get-tuple-element.12.acc_down, bf16[8,3,128,1024]{3,2,1,0:T(8,128)(2,1)S(1)} %get-tuple-element.13.gx, ...), custom_call_target="tpu_custom_call" | custom-call | flops 4294967296 | bytes 33554432 | tf_op jit(solution)/shard_map/pallas_call | solution.py:451

commit v4 on v3

--- a/solution.py
+++ b/solution.py
@@ -354,10 +354,11 @@
         corner(2, sub)
     ready_other(2, 6)
     compute(6)
+    gather(5)
+    weight_grad((5,), acc_up, gx, pg, 0, 1, 2)
     ready_other(3, 7)
     compute(7)
-    gather(5)
-    weight_grad((5,), acc_up, gx, pg)
+    weight_grad((5,), acc_up, gx, pg, 1, 2, 2)
     weight_grad((5,), acc_down, sq, gc)
     gather(6, 7)
     part_copy.wait()

time: 83 us -> 82.6 us (level)
  no operation moved by 1% of the time
where the time goes in v4:
time: 82.6 us; the launch traced here: 82.4 us
  Pallas kernels  81.6 us (99%)
    pallas_call x1, Pallas kernels, few_tokens(): pl.pallas_call(functools.partial(hidden_kernel, reps), out_shape=[pltpu.V...  74.7 us
    pallas_call x1, Pallas kernels, few_tokens(): pl.pallas_call(functools.partial(finish_kernel, reps), out_shape=[jax.Sha...  6.86 us

profile of v4, /device:TPU:0, one launch (start us, length us, event | category | flops | bytes accessed | tf_op | source)
XLA Modules:
  0.0 82.4 jit_solution(16474418738246951232)
XLA Ops:
  0.6 74.7 %shard_map.67 = (f32[1024,2048]{1,0:T(8,128)S(1)}, f32[2048,1024]{1,0:T(8,128)S(1)}, bf16[8,3,128,1024]{3,2,1,0:T(8,128)(2,1)S(1)}, bf16[8,3,128,1024]{3,2,1,0:T...) custom-call(bf16[128,1024]{1,0:T(8,128)(2,1)} %x_ref.1, ...), custom_call_target="tpu_custom_call" | custom-call | flops 30064771072 | bytes 16777216 | tf_op jit(solution)/shard_map/pallas_call | solution.py:426
  75.4 6.9 %shard_map.68 = (bf16[128,1024]{1,0:T(8,128)(2,1)}, f32[1024,2048]{1,0:T(8,128)}, f32[2048,1024]{1,0:T(8,128)}) custom-call(f32[1024,2048]{1,0:T(8,128)S(1)} %get-tuple-element.11.acc_up, f32[2048,1024]{1,0:T(8,128)S(1)} %get-tuple-element.12.acc_down, bf16[8,3,128,1024]{3,2,1,0:T(8,128)(2,1)S(1)} %get-tuple-element.13.gx, ...), custom_call_target="tpu_custom_call" | custom-call | flops 4294967296 | bytes 33554432 | tf_op jit(solution)/shard_map/pallas_call | solution.py:452
